TPU v7x, 32 devices: a whole 2x2x4 slice. The times are simulated.
32 devices in a mesh: sp: 4 (over z), fs: 4 (over y, x), tp: 2 (over core).
Axes of the slice: x: 2, y: 2, z: 4, core: 2. Of those that a mesh axis runs over, the one named last changes fastest.
Arguments:
- tokens: bfloat16 [4, 2048, 2048], P('fs', ('sp', 'tp')), may hold values from -6 to 6
- input_gain: float32 [2048], replicated, may hold values from 0.1 to 1.9
- query_weight: bfloat16 [2048, 768], P(None, 'tp'), may hold values from -0.125 to 0.125
- latent_down: bfloat16 [2048, 256], replicated, may hold values from -0.125 to 0.125
- rotary_down: bfloat16 [2048, 32], replicated, may hold values from -0.125 to 0.125
- pool_down: bfloat16 [2048, 1024], P(None, 'tp'), may hold values from -0.125 to 0.125
- key_up: bfloat16 [256, 512], replicated, may hold values from -0.375 to 0.375
- value_up: bfloat16 [256, 1024], replicated, may hold values from -1.125 to 1.125, as said below
- query_gain: float32 [96], replicated, may hold values from 0.1 to 1.9
- key_gain: float32 [96], replicated, may hold values from 0.1 to 1.9
- pool_weight: bfloat16 [16, 64, 64], replicated, may hold values from -2.25 to 2.25, as said below
- pool_scale: float32 [1024], P('tp'), may hold values from 0.1 to 1.9
- attention_gain: float32 [1024], P('tp'), may hold values from 0.1 to 1.9
- pool_gain: float32 [1024], P('tp'), may hold values from 0.1 to 1.9
- attention_out: bfloat16 [1024, 2048], P('tp'), may hold values from -0.125 to 0.125
- pool_out: bfloat16 [1024, 2048], P('tp'), may hold values from -0.125 to 0.125
Outputs:
- mixed: bfloat16 [4, 2048, 2048], P('fs', ('sp', 'tp'))
Inputs may be any that keep to these rules, and one draw needn't show every extreme that they name: `value_up`: entries of order 256 ** -0.5 or larger. `pool_weight`: entries of order 64 ** -0.5 or larger.
All inputs are finite; a program needn't handle non-finite values.
Results may differ from a plain program's by a relative error of at most 0.015.
Values may be sent and summed in bfloat16 or wider, within the bound.
A program may use at most 64 MiB of HBM per device.

v0:
```python
import math

import jax
import jax.numpy as jnp
from jax import lax
from jax.sharding import PartitionSpec as P

HEADS = 8
NOPE_DIM = 64
ROPE_DIM = 32
VALUE_DIM = 128
KV_LATENT = 256
GROUPS = 16
GROUP_DIM = 64
QK_DIM = 96


EPS = 1e-06
THETA = 10000.0
rim_rows = 16


def passed_along(array, axis, by):
    peers = lax.axis_size(axis)
    pairs = [(i, i + by) for i in range(peers) if 0 <= i + by < peers]
    return lax.ppermute(array, axis, pairs)


def rms_scale(values):
    return lax.rsqrt(jnp.mean(values * values, axis=-1, keepdims=True) + EPS)


def rotate(values, positions):
    half = values.shape[-1] // 2
    inv_freq = 1.0 / THETA ** (jnp.arange(half, dtype=jnp.float32) / half)
    angle = positions[:, None, None] * inv_freq
    cosine = jnp.cos(angle)
    sine = jnp.sin(angle)
    first = values[..., :half]
    second = values[..., half:]
    return jnp.concatenate(
        [first * cosine - second * sine, second * cosine + first * sine], axis=-1
    )


def head_vectors(raw, gain, positions):
    normal = raw * rms_scale(raw) * gain
    turned = rotate(normal[..., NOPE_DIM:], positions)
    return jnp.concatenate([normal[..., :NOPE_DIM], turned], axis=-1).astype(jnp.bfloat16)


def expand_keys(latent_rows, first, key_up, value_up, key_gain):
    count = latent_rows.shape[0]
    heads = key_up.shape[1] // NOPE_DIM
    latent = latent_rows[:, :KV_LATENT].astype(jnp.float32)
    latent_normed = (latent * rms_scale(latent)).astype(jnp.bfloat16)
    plain = jnp.dot(latent_normed, key_up, preferred_element_type=jnp.float32).reshape(
        count, heads, NOPE_DIM
    )
    values = jnp.dot(latent_normed, value_up, preferred_element_type=jnp.float32).astype(
        jnp.bfloat16
    )
    shared = latent_rows[:, KV_LATENT:].astype(jnp.float32)
    shared = jnp.broadcast_to(shared[:, None, :], (count, heads, ROPE_DIM))
    positions = (first + jnp.arange(count, dtype=jnp.int32)).astype(jnp.float32)
    keys = head_vectors(jnp.concatenate([plain, shared], axis=-1), key_gain, positions)
    return (keys, values.reshape(count, heads, VALUE_DIM))


def attend(state, queries, keys, values, query_pos, key_pos):
    numer, denom = state
    scores = jnp.einsum("qhd,khd->hqk", queries, keys, preferred_element_type=jnp.float32)
    scores = scores * (1.0 / math.sqrt(QK_DIM))
    visible = key_pos[None, None, :] <= query_pos[None, :, None]
    weights = jnp.where(visible, jnp.exp(scores), 0.0)
    numer = numer + jnp.einsum(
        "hqk,khd->qhd", weights.astype(jnp.bfloat16), values, preferred_element_type=jnp.float32
    )
    denom = denom + jnp.sum(weights, axis=-1)
    return (numer, denom)


def keep_state(current):
    return current


def pool_mix(pool_input, before, group_ids, positions):
    count = pool_input.shape[0]
    groups = group_ids.shape[0]
    current = pool_input.astype(jnp.float32).reshape(count, groups, GROUP_DIM)
    extended = jnp.concatenate([before, pool_input], axis=0).astype(jnp.float32)
    extended = extended.reshape(count + rim_rows, groups, GROUP_DIM)
    window = jnp.left_shift(2, group_ids % 4).astype(jnp.float32)
    total = current
    for back in range(1, rim_rows):
        taken = (window > back).astype(jnp.float32)
        total = total + extended[rim_rows - back : rim_rows - back + count] * taken[None, :, None]
    divisor = jnp.minimum(positions[:, None] + 1.0, window[None, :])
    return (total / divisor[:, :, None] - current).astype(jnp.bfloat16)


def local(
    tokens,
    input_gain,
    query_weight,
    latent_down,
    rotary_down,
    pool_down,
    key_up,
    value_up,
    query_gain,
    key_gain,
    pool_weight,
    pool_scale,
    attention_gain,
    pool_gain,
    attention_out,
    pool_out,
):
    width_tp = lax.axis_size("tp")
    block = tokens.shape[1] * width_tp
    heads = HEADS // width_tp
    groups = GROUPS // width_tp
    member = lax.axis_index("tp")
    own_key_up = lax.dynamic_slice_in_dim(key_up, member * heads * NOPE_DIM, heads * NOPE_DIM, 1)
    own_value_up = lax.dynamic_slice_in_dim(
        value_up, member * heads * VALUE_DIM, heads * VALUE_DIM, 1
    )
    own_pool_weight = lax.dynamic_slice_in_dim(pool_weight, member * groups, groups, 0)
    source = tokens[0].astype(jnp.float32)
    normed = (source * rms_scale(source) * input_gain).astype(jnp.bfloat16)
    offset = lax.axis_index("sp") * block
    positions_int = offset + jnp.arange(block, dtype=jnp.int32)
    positions = positions_int.astype(jnp.float32)
    latent_width = KV_LATENT + ROPE_DIM
    query_width = heads * QK_DIM
    piece = lax.all_gather(normed, "tp", axis=0, tiled=True)
    projected = jnp.concatenate(
        [
            jnp.dot(piece, latent_down, preferred_element_type=jnp.float32),
            jnp.dot(piece, rotary_down, preferred_element_type=jnp.float32),
            jnp.dot(piece, query_weight, preferred_element_type=jnp.float32),
            jnp.dot(piece, pool_down, preferred_element_type=jnp.float32),
        ],
        axis=1,
    )
    latent_rows = projected[:, :latent_width].astype(jnp.bfloat16)
    query_raw = projected[:, latent_width : latent_width + query_width]
    pool_input = projected[:, latent_width + query_width :].astype(jnp.bfloat16)
    pool_channels = pool_input.shape[1]
    rim = pool_input[block - rim_rows :].reshape(-1, 128)
    before = passed_along(rim, "sp", 1).reshape(rim_rows, pool_channels)
    queries = head_vectors(query_raw.reshape(block, heads, QK_DIM), query_gain, positions)
    last_query = offset + block - 1
    start_state = (
        jnp.zeros((block, heads, VALUE_DIM), jnp.float32),
        jnp.zeros((heads, block), jnp.float32),
    )
    own_keys, own_values = expand_keys(latent_rows, offset, own_key_up, own_value_up, key_gain)
    flat_keys = own_keys.reshape(block, heads * QK_DIM)
    flat_values = own_values.reshape(block, heads * VALUE_DIM)
    piece_keys = lax.all_gather(flat_keys, "sp", axis=0, tiled=True)
    piece_values = lax.all_gather(flat_values, "sp", axis=0, tiled=True)

    def one_block(index, inner):
        first = index * block

        def work(current):
            keys = lax.dynamic_slice_in_dim(piece_keys, index * block, block, 0)
            values = lax.dynamic_slice_in_dim(piece_values, index * block, block, 0)
            key_pos = first + jnp.arange(block, dtype=jnp.int32)
            return attend(
                current,
                queries,
                keys.reshape(block, heads, QK_DIM),
                values.reshape(block, heads, VALUE_DIM),
                positions_int,
                key_pos,
            )

        return lax.cond(first <= last_query, work, keep_state, inner)

    numer, denom = lax.fori_loop(0, piece_keys.shape[0] // block, one_block, start_state)
    attended = (numer / jnp.transpose(denom)[:, :, None]).reshape(block, heads * VALUE_DIM)
    group_ids = member * groups + jnp.arange(groups, dtype=jnp.int32)
    pooled_mean = pool_mix(pool_input, before, group_ids, positions)
    pooled = jnp.einsum(
        "rgc,gcd->rgd", pooled_mean, own_pool_weight, preferred_element_type=jnp.float32
    )
    pooled = pooled.reshape(block, pool_channels) * pool_scale
    attention_total, pool_total = lax.psum(
        (jnp.sum(attended * attended, axis=1), jnp.sum(pooled * pooled, axis=1)), "tp"
    )
    attention_factor = lax.rsqrt(attention_total / (HEADS * VALUE_DIM) + EPS)
    pool_factor = lax.rsqrt(pool_total / (GROUPS * GROUP_DIM) + EPS)
    attention_mixed = (attended * attention_factor[:, None] * attention_gain).astype(jnp.bfloat16)
    pool_mixed = (pooled * pool_factor[:, None] * pool_gain).astype(jnp.bfloat16)
    term = jnp.dot(attention_mixed, attention_out, preferred_element_type=jnp.float32)
    summed = lax.psum_scatter(
        (term + jnp.dot(pool_mixed, pool_out, preferred_element_type=jnp.float32)).astype(
            jnp.bfloat16
        ),
        "tp",
        scatter_dimension=0,
        tiled=True,
    )
    return summed[None]


def solution(mesh):
    placed = (
        P("fs", ("sp", "tp"), None),
        P(),
        P(None, "tp"),
        P(),
        P(),
        P(None, "tp"),
        P(),
        P(),
        P(),
        P(),
        P(),
        P("tp"),
        P("tp"),
        P("tp"),
        P("tp", None),
        P("tp", None),
    )
    return jax.shard_map(
        local, mesh=mesh, in_specs=placed, out_specs=P("fs", ("sp", "tp"), None), check_vma=False
    )
```

profile of v0, /device:TPU:25, one launch (start us, length us, event | category | flops | bytes accessed | tf_op | source)
XLA Modules:
  0.0 156.7 jit_solution(11818657221322696998)
XLA Ops:
  13.7 9.5 %all-gather.4.cloned.1.call-done = bf16[512,2048]{1,0:T(8,128)(2,1)} async-done(((bf16[256,2048]{1,0:T(8,128)(2,1)}), bf16[512,2048]{1,0:T(8,128)(2,1)}) %all-gather.4.cloned.1.call-update) | async-done | bytes 2097168 | tf_op jit(solution)/shard_map/all_gather | solution.py:137
  23.2 2.6 %multiply_reduce_fusion.3 = (f32[512]{0:T(512)S(1)}, f32[512,256]{0,1:T(8,128)S(1)}) fusion(bf16[512,2048]{1,0:T(8,128)(2,1)} %all-gather.4.cloned.1.call-done, bf16[2048,256]{1,0:T(8,128)(2,1)} %param.23), kind=kOutput, calls=%fused_computation.51 | convolution fusion | flops 537394688 | bytes 3672064 | tf_op jit(solution)/shard_map/dot_general | solution.py:140
  37.5 3.5 %convolution_convert_fusion = bf16[512,512]{1,0:T(8,128)(2,1)S(1)} fusion(bf16[512,2048]{1,0:T(8,128)(2,1)} %all-gather.4.cloned.1.call-done, bf16[2048,512]{1,0:T(8,128)(2,1)} %param.25), kind=kOutput, calls=%fused_computation.23 | convolution fusion | flops 1074003968 | bytes 4718592 | tf_op jit(solution)/shard_map/dot_general | solution.py:143
  45.2 4.3 %collective-permute-done = bf16[64,128]{1,0:T(8,128)(2,1)} collective-permute-done((bf16[64,128]{1,0:T(8,128)(2,1)}, bf16[64,128]{1,0:T(8,128)(2,1)}, u32[]{:S(2)}, u32[]{:S(2)}) %collective-permute-start) | collective-permute-done | bytes 16416 | tf_op jit(solution)/shard_map/ppermute | solution.py:26
  52.0 5.6 %fusion.40 = (f32[512,512]{1,0:T(8,128)}, f32[512,512]{1,0:T(8,128)}, f32[512,512]{1,0:T(8,128)}, f32[512,512]{1,0:T(8,128)}, f32[512,512]{1,0:T(8,128)}, /*inde...) fusion(f32[528,512]{1,0:T(8,128)S(1)} %maximum_convert_fusion), kind=kLoop, calls=%fused_computation.99 | loop fusion | bytes 31457280 | tf_op jit(solution)/shard_map/slice | solution.py:97
  57.7 2.6 %copy.55 = f32[512,512]{0,1:T(8,128)} copy(f32[512,512]{1,0:T(8,128)} %get-tuple-element.246) | data formatting | bytes 2097152 | tf_op jit(solution)/shard_map/slice | solution.py:97
  65.3 2.6 %copy.52 = f32[512,512]{0,1:T(8,128)} copy(f32[512,512]{1,0:T(8,128)} %get-tuple-element.249) | data formatting | bytes 2097152 | tf_op jit(solution)/shard_map/slice | solution.py:97
  75.5 2.6 %copy.48 = f32[512,512]{0,1:T(8,128)} copy(f32[512,512]{1,0:T(8,128)} %get-tuple-element.253) | data formatting | bytes 2097152 | tf_op jit(solution)/shard_map/slice | solution.py:97
  80.6 2.6 %copy.46 = f32[512,512]{0,1:T(8,128)} copy(f32[512,512]{1,0:T(8,128)} %get-tuple-element.255) | data formatting | bytes 2097152 | tf_op jit(solution)/shard_map/slice | solution.py:97
  83.2 2.6 %copy.45 = f32[512,512]{0,1:T(8,128)} copy(f32[512,512]{1,0:T(8,128)} %get-tuple-element.256) | data formatting | bytes 2097152 | tf_op jit(solution)/shard_map/slice | solution.py:97
  85.8 2.5 %copy.44 = f32[512,512]{0,1:T(8,128)} copy(f32[512,512]{1,0:T(8,128)} %get-tuple-element.257) | data formatting | bytes 2097152 | tf_op jit(solution)/shard_map/slice | solution.py:97
  88.3 2.6 %copy.43 = f32[512,512]{0,1:T(8,128)} copy(f32[512,512]{1,0:T(8,128)} %get-tuple-element.258) | data formatting | bytes 2097152 | tf_op jit(solution)/shard_map/slice | solution.py:97
  90.9 2.6 %copy.42 = f32[512,512]{0,1:T(8,128)} copy(f32[512,512]{1,0:T(8,128)} %get-tuple-element.259) | data formatting | bytes 2097152 | tf_op jit(solution)/shard_map/slice | solution.py:97
  93.5 2.5 %copy.41 = f32[512,512]{0,1:T(8,128)} copy(f32[512,512]{1,0:T(8,128)} %get-tuple-element.245) | data formatting | bytes 2097152 | tf_op jit(solution)/shard_map/slice | solution.py:97
  96.0 9.0 %fusion.26 = (f32[512]{0:T(512)}, f32[8,64,512]{2,1,0:T(8,128)}) fusion(f32[8,64]{1,0:T(8,128)S(1)} %mul.425, f32[512,8,64]{0,2,1:T(8,128)S(1)} %bitcast.82, f32[512,8,64]{0,2,1:T(8,128)} %bitcast.83, f32[512,8,64]{0,2,1:T(8,128)} %bitcast.84, f32[512,8,64]{0,2,1:T(8,128)} %bitcast.85, f32[512,8,64]{0,2,1:T(8,128)} %bitcast.86, f32[512,8,64]{0,2,1:T(8,128)} %bitcast.87, ...), kind=kOutput, calls=%fused_computation.35 | convolution fusion | flops 42991104 | bytes 17984068 | tf_op jit(solution)/shard_map/rgc,gcd->rgd/dot_general | solution.py:187
  105.0 4.0 %copy.38 = bf16[2048,512]{0,1:T(8,128)(2,1)} copy(bf16[2048,512]{1,0:T(8,128)(2,1)} %all-gather.6.cloned.1.call-done) | data formatting | bytes 4194304
  109.0 19.7 %while.16 = (s32[]{:T(128)}, f32[512,4,128]{0,2,1:T(8,128)S(1)}, f32[4,512]{1,0:T(4,128)S(1)}, s32[]{:T(128)}, bf16[2048,512]{0,1:T(8,128)(2,1)}, /*index=5*/bf1...) while((s32[]{:T(128)}, f32[512,4,128]{0,2,1:T(8,128)S(1)}, ...), condition=%wide.region_8.9_spmd.clone, body=%wide.region_4.8_spmd.clone.sunk | while | flops 476578816 | bytes 14463285 | solution.py:183
  109.1 4.9 %conditional.3 = ((f32[512,4,128]{0,2,1:T(8,128)S(1)}, f32[4,512]{1,0:T(4,128)S(1)})) conditional(s32[]{:T(128)} %convert_element_type.332, (f32[512,4,128]{0,2,1:T(8,128)S(1)}, f32[4,512]{1,0:T(4,128)S(1)}) %tuple.76, (s32[]{:T(128)}, bf16[2048,512]{0,1:T(8,128)(2,1)}, s32[]{:T(128)}, s32[]{:T(128)}, bf16[2048,384]{0,1:T(8,128)(2,1)}, ...), branch_computations={%region_5.0_spmd, %region_6.7_spmd} | conditional | flops 476578816 | bytes 14461014 | solution.py:181
  114.0 4.9 %conditional.3 = ((f32[512,4,128]{0,2,1:T(8,128)S(1)}, f32[4,512]{1,0:T(4,128)S(1)})) conditional(s32[]{:T(128)} %convert_element_type.332, (f32[512,4,128]{0,2,1:T(8,128)S(1)}, f32[4,512]{1,0:T(4,128)S(1)}) %tuple.76, (s32[]{:T(128)}, bf16[2048,512]{0,1:T(8,128)(2,1)}, s32[]{:T(128)}, s32[]{:T(128)}, bf16[2048,384]{0,1:T(8,128)(2,1)}, ...), branch_computations={%region_5.0_spmd, %region_6.7_spmd} | conditional | flops 476578816 | bytes 14461014 | solution.py:181
  118.9 4.9 %conditional.3 = ((f32[512,4,128]{0,2,1:T(8,128)S(1)}, f32[4,512]{1,0:T(4,128)S(1)})) conditional(s32[]{:T(128)} %convert_element_type.332, (f32[512,4,128]{0,2,1:T(8,128)S(1)}, f32[4,512]{1,0:T(4,128)S(1)}) %tuple.76, (s32[]{:T(128)}, bf16[2048,512]{0,1:T(8,128)(2,1)}, s32[]{:T(128)}, s32[]{:T(128)}, bf16[2048,384]{0,1:T(8,128)(2,1)}, ...), branch_computations={%region_5.0_spmd, %region_6.7_spmd} | conditional | flops 476578816 | bytes 14461014 | solution.py:181
  123.8 4.9 %conditional.3 = ((f32[512,4,128]{0,2,1:T(8,128)S(1)}, f32[4,512]{1,0:T(4,128)S(1)})) conditional(s32[]{:T(128)} %convert_element_type.332, (f32[512,4,128]{0,2,1:T(8,128)S(1)}, f32[4,512]{1,0:T(4,128)S(1)}) %tuple.76, (s32[]{:T(128)}, bf16[2048,512]{0,1:T(8,128)(2,1)}, s32[]{:T(128)}, s32[]{:T(128)}, bf16[2048,384]{0,1:T(8,128)(2,1)}, ...), branch_computations={%region_5.0_spmd, %region_6.7_spmd} | conditional | flops 476578816 | bytes 14461014 | solution.py:181
  129.9 3.0 %all-reduce = (f32[512]{0:T(512)S(1)}, f32[512]{0:T(512)S(1)}) all-reduce(f32[512]{0:T(512)S(1)} %get-tuple-element.239, f32[512]{0:T(512)S(1)} %copy-done.11), channel_id=1, replica_groups=mesh['sp'=4,'fs'=4,'tp'=2] {'tp'}, use_global_device_ids=true, to_apply=%region_10.11 | all-reduce | flops 1024 | bytes 8192 | tf_op jit(solution)/shard_map/psum | solution.py:191
  136.2 2.7 %add_convert_fusion = bf16[512,2048]{1,0:T(8,128)(2,1)} fusion(f32[512,2048]{1,0:T(8,128)S(1)} %fusion.42, bf16[512,512]{0,1:T(8,128)(2,1)S(1)} %fusion.24, bf16[512,2048]{1,0:T(8,128)(2,1)S(1)} %copy-done.4), kind=kOutput, calls=%fused_computation.17 | convolution fusion | flops 1075838976 | bytes 8912896 | tf_op jit(solution)/shard_map/dot_general | solution.py:200
  139.0 11.2 %reduce-scatter.2.cloned.1.call-done = bf16[256,2048]{1,0:T(8,128)(2,1)} async-done(((bf16[512,2048]{1,0:T(8,128)(2,1)}), bf16[256,2048]{1,0:T(8,128)(2,1)}) %reduce-scatter.2.cloned.1.call-update) | async-done | bytes 1048592 | tf_op jit(solution)/shard_map/reduce_scatter | solution.py:199
  (136 shorter events, 64.3 us)
Async XLA Ops:
  6.5 127.8 %copy-start = (bf16[512,2048]{1,0:T(8,128)(2,1)S(1)}, bf16[512,2048]{1,0:T(8,128)(2,1)}, u32[]{:S(2)}) copy-start(bf16[512,2048]{1,0:T(8,128)(2,1)} %param.34) | copy-start | bytes 6291460
  6.5 4.3 %copy-start.10 = (f32[512]{0:T(512)S(1)}, f32[512]{0:T(512)}, u32[]{:S(2)}) copy-start(f32[512]{0:T(512)} %param.31) | copy-start | bytes 6148
  6.5 16.6 %all-gather.4.cloned.1.call-start = ((), (), s32[]{:S(2)}) async-start(), calls=%async_computation.1 | async-start | bytes 3145728 | tf_op jit(solution)/shard_map/all_gather | solution.py:137
  10.8 15.1 %copy-start.7 = (bf16[256,1024]{1,0:T(8,128)(2,1)S(1)}, bf16[256,1024]{1,0:T(8,128)(2,1)}, u32[]{:S(2)}) copy-start(bf16[256,1024]{1,0:T(8,128)(2,1)} %param.27) | copy-start | bytes 1572868
  10.8 94.2 %all-gather.6.cloned.1.call-start = ((), (), s32[]{:S(2)}) async-start(), calls=%async_computation.2 | async-start | bytes 2621440 | tf_op jit(solution)/shard_map/all_gather | solution.py:163
  13.7 17.1 %copy-start.9 = (bf16[256,512]{1,0:T(8,128)(2,1)S(1)}, bf16[256,512]{1,0:T(8,128)(2,1)}, u32[]{:S(2)}) copy-start(bf16[256,512]{1,0:T(8,128)(2,1)} %param.26) | copy-start | bytes 786436
  25.8 5.3 %copy-start.8 = (bf16[2048,32]{0,1:T(8,128)(2,1)S(1)}, bf16[2048,32]{0,1:T(8,128)(2,1)}, u32[]{:S(2)}) copy-start(bf16[2048,32]{0,1:T(8,128)(2,1)} %param.24) | copy-start | bytes 393220
  27.0 81.9 %all-gather.8.cloned.1.call-start = ((), (), s32[]{:S(2)}) async-start(), calls=%async_computation.3 | async-start | bytes 1966080 | tf_op jit(solution)/shard_map/all_gather | solution.py:162
  30.8 2.9 %copy-start.3 = (bf16[512,2048]{1,0:T(8,128)(2,1)S(1)}, bf16[512,2048]{1,0:T(8,128)(2,1)}, u32[]{:S(2)}) copy-start(bf16[512,2048]{1,0:T(8,128)(2,1)} %all-gather.4.cloned.1.call-done) | copy-start | bytes 6291460
  30.8 2.9 %copy-start.19 = (bf16[2048,384]{1,0:T(8,128)(2,1)S(1)}, bf16[2048,384]{1,0:T(8,128)(2,1)}, u32[]{:S(2)}) copy-start(bf16[2048,384]{1,0:T(8,128)(2,1)} %param.22) | copy-start | bytes 4718596
  33.7 1.2 copy-start.14
  33.7 1.2 copy-start.15
  34.9 1.8 %copy-start.18 = (f32[8]{0:T(128)S(1)}, f32[8]{0:T(128)}, u32[]{:S(2)}) copy-start(f32[8]{0:T(128)} %fusion.38) | copy-start | bytes 100
  36.7 113.4 %reduce-scatter.2.cloned.1.call-start = ((), (), s32[]{:S(2)}) async-start(), calls=%async_computation.4 | async-start | bytes 3145728 | tf_op jit(solution)/shard_map/reduce_scatter | solution.py:199
  37.5 6.4 %copy-start.5 = (bf16[512,4,16]{0,2,1:T(8,128)(2,1)S(1)}, bf16[512,4,16]{0,2,1:T(8,128)(2,1)}, u32[]{:S(2)}) copy-start(bf16[512,4,16]{0,2,1:T(8,128)(2,1)} %get-tuple-element.260) | copy-start | bytes 196612
  37.5 6.4 %copy-start.6 = (bf16[512,4,16]{0,2,1:T(8,128)(2,1)S(1)}, bf16[512,4,16]{0,2,1:T(8,128)(2,1)}, u32[]{:S(2)}) copy-start(bf16[512,4,16]{0,2,1:T(8,128)(2,1)} %get-tuple-element.261) | copy-start | bytes 196612
  42.5 7.1 %collective-permute-start = (bf16[64,128]{1,0:T(8,128)(2,1)}, bf16[64,128]{1,0:T(8,128)(2,1)}, u32[]{:S(2)}, u32[]{:S(2)}) collective-permute-start(bf16[64,128]{1,0:T(8,128)(2,1)} %reshape.332), channel_id=1, source_target_pairs={{0,8},{8,16},{16,24},{1,9},{9,17},{17,25},{2,10},{10,18},{18,26},{... | collective-permute-start | bytes 49160 | tf_op jit(solution)/shard_map/ppermute | solution.py:26
  90.9 5.1 %copy-start.16 = (f32[8]{0:T(128)S(1)}, f32[8]{0:T(128)}, u32[]{:S(2)}) copy-start(f32[8]{0:T(128)} %get-tuple-element.272) | copy-start | bytes 100
  90.9 5.1 %copy-start.17 = (f32[8]{0:T(128)S(1)}, f32[8]{0:T(128)}, u32[]{:S(2)}) copy-start(f32[8]{0:T(128)} %get-tuple-element.273) | copy-start | bytes 100
  128.7 1.2 copy-start.11
  128.7 4.2 %copy-start.12 = (f32[512]{0:T(512)S(1)}, f32[512]{0:T(512)}, u32[]{:S(2)}) copy-start(f32[512]{0:T(512)} %param.32) | copy-start | bytes 6148
  134.3 1.3 copy-start.1
  134.3 1.3 copy-start.13
  134.3 1.9 %copy-start.4 = (bf16[512,2048]{1,0:T(8,128)(2,1)S(1)}, bf16[512,2048]{1,0:T(8,128)(2,1)}, u32[]{:S(2)}) copy-start(bf16[512,2048]{1,0:T(8,128)(2,1)} %param.35) | copy-start | bytes 6291460
  (1 other events, 0.8 us)
Sparse Core Ops, SparseCore 0:
  10.9 12.2 all-gather.3
  27.1 44.6 all-gather.5
  73.4 35.4 all-gather.7
  139.1 11.0 reduce-scatter.1
where the time goes:
time: 159 us; the launch traced here: 157 us
  local copies, waits for them, and re-layouts  61.1 us (38%)
  matrix products  33.9 us (21%)
  waiting for transfers between devices  25 us (16%)
  other arithmetic  18.1 us (11%)
  between operations  13.5 us (8%)
  blocking collectives  3.01 us (2%)
  starting transfers between devices  1.59 us (1%)
    slice x16, local copies, waits for them, and re-layouts, pool_mix(): extended[rim_rows - back:rim_rows - back + count] * taken[None, :, None]  43.9 us
    reduce_scatter x1, waiting for transfers between devices, local(): lax.psum_scatter((term + jnp.dot(pool_mixed, pool_out, preferred_element_...  11.2 us
    all_gather x1, waiting for transfers between devices, local(): piece = lax.all_gather(normed, 'tp', axis=0, tiled=True)  9.48 us
    dot_general x1, matrix products, local(): jnp.einsum('rgc,gcd->rgd', pooled_mean, own_pool_weight, preferred_elemen...  8.95 us
    dot_general x4, matrix products, attend(): jnp.einsum('qhd,khd->hqk', queries, keys, preferred_element_type=jnp.floa...  5.35 us
    unnamed x41, local copies, waits for them, and re-layouts  5.2 us
    convert_element_type x8, other arithmetic, pool_mix(): taken = (window > back).astype(jnp.float32)  4.64 us
    dot_general x4, matrix products, attend(): jnp.einsum('hqk,khd->qhd', weights.astype(jnp.bfloat16), values, preferre...  4.56 us
  transfers between devices with their start and end apart: 5, of which 3 were waited for; matrix products, arithmetic and copies ran while one was open for 50% of the time, Pallas kernels for 0%

commit v1 on v0

v1 whole, which is shorter than its diff:
```python
import functools
import math

import jax
import jax.numpy as jnp
import numpy as np
from jax import lax
from jax.experimental import pallas as pl
from jax.experimental.pallas import tpu as pltpu
from jax.sharding import PartitionSpec as P

HEADS = 8
NOPE_DIM = 64
ROPE_DIM = 32
VALUE_DIM = 128
KV_LATENT = 256
GROUPS = 16
GROUP_DIM = 64
QK_DIM = 96
EPS = 1e-06
THETA = 10000.0
RIM = 16
HALF = ROPE_DIM // 2
MESH = pl.DeviceIdType.MESH
F32 = jnp.float32
BF16 = jnp.bfloat16


def dot(a, b):
    return jnp.dot(a, b, preferred_element_type=F32)


def column_of(row, width):
    return jnp.transpose(jnp.broadcast_to(row, (128, width)))[:, :1]


def kernel(
    sp, tp,
    tokens_h, input_gain_h, query_w_h, latent_w_h, rotary_w_h, pool_w_h, key_up_h, value_up_h,
    query_gain_h, key_gain_h, mix_w_h, scale_h, att_gain_h, pool_gain_h, att_out_h, pool_out_h,
    cos_h, sin_h,
    out_ref,
    x_all, input_gain, query_w, latent_w, rotary_w, pool_w, key_up, value_up,
    query_gain, key_gain, mix_w, scale, att_gain, pool_gain, att_out, pool_out, cos_t, sin_t,
    normed, key_up_t, lat_buf, rot_buf, queries, keys_t, vals, acc, ext, rim_out, rim_in, blockdiag,
    pooled_ref, acc_pool, ss_buf, mixed, send_buf, recv_buf,
    load_sem, tok_send, tok_recv, z_send, z_recv, f_send, f_recv, rim_send, rim_recv,
    ss_send, ss_recv, out_send, out_recv,
):
    s = lax.axis_index("sp")
    m = lax.axis_index("tp")
    rows, width = tokens_h.shape
    block = rows * tp
    heads = HEADS // tp
    groups = GROUPS // tp
    chans = groups * GROUP_DIM
    chunks, _, _, cw = send_buf.shape

    def peer(j):
        return lax.rem(m + j, tp)

    def load(i, src, dst):
        return pltpu.make_async_copy(src, dst, load_sem.at[i])

    loads = {
        "x": load(0, tokens_h, x_all.at[m]),
        "ig": load(1, input_gain_h, input_gain),
        "lw": load(2, latent_w_h, latent_w),
        "rw": load(3, rotary_w_h, rotary_w),
        "pw": load(4, pool_w_h, pool_w),
        "qw": load(5, query_w_h, query_w),
        "qg": load(6, query_gain_h, query_gain),
        "kg": load(7, key_gain_h, key_gain),
        "cos": load(8, cos_h, cos_t),
        "sin": load(9, sin_h, sin_t),
        "ku": load(10, key_up_h, key_up),
        "vu": load(11, value_up_h.at[:, pl.ds(pl.multiple_of(m * heads * VALUE_DIM, 128), heads * VALUE_DIM)], value_up),
        "mw": load(12, mix_w_h.at[pl.ds(m * groups, groups)], mix_w),
        "sc": load(13, scale_h, scale),
        "pg": load(14, pool_gain_h, pool_gain),
        "po": load(15, pool_out_h, pool_out),
        "ag": load(16, att_gain_h, att_gain),
        "ao": load(17, att_out_h, att_out),
    }
    for item in loads.values():
        item.start()

    barrier = pltpu.get_barrier_semaphore()
    for j in range(1, tp):
        pl.semaphore_signal(barrier, inc=1, device_id={"tp": peer(j)}, device_id_type=MESH)
    for d in range(1, sp):
        pl.semaphore_signal(barrier, inc=1, device_id={"sp": lax.rem(s + d, sp)}, device_id_type=MESH)
    pl.semaphore_wait(barrier, tp - 1 + sp - 1)

    def remote(src, dst, ssem, rsem, where):
        return pltpu.make_async_remote_copy(
            src_ref=src, dst_ref=dst, send_sem=ssem, recv_sem=rsem, device_id=where, device_id_type=MESH
        )

    def tok_copy(j, owner):
        return remote(tokens_h, x_all.at[owner], tok_send.at[j], tok_recv.at[owner], {"tp": peer(j)})

    def z_copy(d, src):
        where = {"sp": lax.rem(s + d, sp)}
        return [
            remote(buf.at[src, m], buf.at[src, m], z_send.at[d, k], z_recv.at[src, k], where)
            for k, buf in enumerate((lat_buf, rot_buf))
        ]

    def f_copy(src, j, owner):
        where = {"tp": peer(j)}
        return [
            remote(buf.at[src, owner], buf.at[src, owner], f_send.at[src, j, k], f_recv.at[src, owner, k], where)
            for k, buf in enumerate((lat_buf, rot_buf))
        ]

    def rim_copy():
        return remote(rim_out, rim_in, rim_send.at[0], rim_recv.at[0], {"sp": lax.rem(s + 1, sp)})

    def ss_copy(k, j, owner):
        return remote(ss_buf.at[k, owner], ss_buf.at[k, owner], ss_send.at[k, j], ss_recv.at[k, owner], {"tp": peer(j)})

    def out_copy(c, j, owner):
        return remote(send_buf.at[c, peer(j)], recv_buf.at[c, owner], out_send.at[c, j], out_recv.at[c, owner], {"tp": peer(j)})

    for j in range(1, tp):
        tok_copy(j, m).start()

    step = min(64, rows)

    def norm_piece(piece):
        def body(i, carry):
            at = pl.multiple_of(i * step, step)
            x = x_all[piece, pl.ds(at, step), :].astype(F32)
            r = lax.rsqrt(jnp.mean(x * x, axis=-1, keepdims=True) + EPS)
            normed[piece, pl.ds(at, step), :] = (x * r * input_gain[...]).astype(BF16)
            return carry

        lax.fori_loop(0, rows // step, body, 0)

    loads["x"].wait()
    loads["ig"].wait()
    norm_piece(m)
    loads["lw"].wait()
    loads["rw"].wait()
    own = normed[m]
    lat_buf[s, m] = dot(own, latent_w[...]).astype(BF16)
    rot = dot(own, rotary_w[...])
    rot = jnp.concatenate([rot, jnp.zeros((rows, 128 - ROPE_DIM), F32)], axis=1)
    rot_buf[s, m] = jnp.transpose(rot)[:ROPE_DIM].astype(BF16)
    for d in range(1, sp):
        @pl.when(s + d < sp)
        def _():
            for c in z_copy(d, s):
                c.start()
    for j in range(1, tp):
        for c in f_copy(s, j, m):
            c.start()

    for j in range(1, tp):
        tok_copy(j, peer(j)).wait_recv()
        norm_piece(peer(j))

    full = normed[...].reshape(block, width)
    loads["pw"].wait()
    pool_in = dot(full, pool_w[...]).astype(BF16)
    ext[RIM:, :] = pool_in.astype(F32)
    rim_out[...] = pool_in[block - RIM :, :]

    @pl.when(s + 1 < sp)
    def _():
        rim_copy().start()

    loads["qw"].wait()
    loads["qg"].wait()
    loads["cos"].wait()
    loads["sin"].wait()
    query_t = jnp.transpose(dot(full, query_w[...]))
    factor = math.log2(math.e) / math.sqrt(QK_DIM)
    gain_q = column_of(query_gain[...], QK_DIM) * factor
    at = pl.multiple_of(s * block, 128)
    cosine = cos_t[:, pl.ds(at, block)]
    sine = sin_t[:, pl.ds(at, block)]
    pad = jnp.zeros((128 - QK_DIM, block), F32)
    for h in range(heads):
        u = query_t[h * QK_DIM : (h + 1) * QK_DIM]
        r = lax.rsqrt(jnp.sum(u * u, axis=0, keepdims=True) * (1.0 / QK_DIM) + EPS)
        n = u * r * gain_q
        a = n[NOPE_DIM : NOPE_DIM + HALF]
        b = n[NOPE_DIM + HALF :]
        turned = jnp.concatenate(
            [n[:NOPE_DIM], a * cosine - b * sine, b * cosine + a * sine, pad], axis=0
        )
        queries[h] = jnp.transpose(turned).astype(BF16)

    loads["ku"].wait()
    key_up_t[...] = jnp.transpose(key_up[...].astype(F32)).astype(BF16)
    loads["kg"].wait()
    gain_k = column_of(key_gain[...], QK_DIM)
    gain_k_plain = gain_k[:NOPE_DIM]
    gain_k_rot = gain_k[NOPE_DIM:]
    loads["vu"].wait()
    for h in range(heads):
        keys_t[h, QK_DIM:, :] = jnp.zeros((128 - QK_DIM, block), BF16)
        vals[h, :, VALUE_DIM:] = jnp.ones((block, VALUE_DIM), BF16)

    def expand(src):
        latent = lat_buf[src].reshape(block, KV_LATENT).astype(F32)
        r = lax.rsqrt(jnp.mean(latent * latent, axis=-1, keepdims=True) + EPS)
        latent_normed = (latent * r).astype(BF16)
        own_up = key_up_t[pl.ds(pl.multiple_of(m * heads * NOPE_DIM, 64), heads * NOPE_DIM), :]
        plain = lax.dot_general(
            own_up, latent_normed, (((1,), (1,)), ((), ())), preferred_element_type=F32
        )
        value = dot(latent_normed, value_up[...]).astype(BF16)
        pieces = [rot_buf[src, j].astype(F32) for j in range(tp)]
        shared = jnp.concatenate(pieces, axis=1) if tp > 1 else pieces[0]
        shared_sum = jnp.sum(shared * shared, axis=0, keepdims=True)
        first = pl.multiple_of(src * block, 128)
        cosine = cos_t[:, pl.ds(first, block)]
        sine = sin_t[:, pl.ds(first, block)]
        scaled = shared * gain_k_rot
        a = scaled[:HALF]
        b = scaled[HALF:]
        turned_a = a * cosine - b * sine
        turned_b = b * cosine + a * sine
        for h in range(heads):
            u = plain[h * NOPE_DIM : (h + 1) * NOPE_DIM]
            total = jnp.sum(u * u, axis=0, keepdims=True) + shared_sum
            r = lax.rsqrt(total * (1.0 / QK_DIM) + EPS)
            keys_t[h, :NOPE_DIM, :] = (u * gain_k_plain * r).astype(BF16)
            keys_t[h, NOPE_DIM : NOPE_DIM + HALF, :] = (turned_a * r).astype(BF16)
            keys_t[h, NOPE_DIM + HALF : QK_DIM, :] = (turned_b * r).astype(BF16)
            vals[h, :, :VALUE_DIM] = value[:, h * VALUE_DIM : (h + 1) * VALUE_DIM]

    qc = min(256, block)

    def attend(head, diagonal):
        for q0 in range(0, block, qc):
            span = q0 + qc if diagonal else block
            score = dot(queries[head, q0 : q0 + qc, :], keys_t[head, :, :span])
            weight = jnp.exp2(score)
            if diagonal:
                qpos = q0 + lax.broadcasted_iota(jnp.int32, (qc, span), 0)
                kpos = lax.broadcasted_iota(jnp.int32, (qc, span), 1)
                weight = jnp.where(kpos <= qpos, weight, 0.0)
            got = dot(weight.astype(BF16), vals[head, :span, :])
            if diagonal:
                acc[head, q0 : q0 + qc, :] = got
            else:
                acc[head, q0 : q0 + qc, :] += got

    for name in ("mw", "sc", "pg"):
        loads[name].wait()
    blockdiag[...] = jnp.zeros((chans, chans), BF16)
    for g in range(groups):
        lo = g * GROUP_DIM
        blockdiag[lo : lo + GROUP_DIM, lo : lo + GROUP_DIM] = mix_w[g]

    @pl.when(s > 0)
    def _():
        rim_copy().wait_recv()
        ext[:RIM, :] = rim_in[...].astype(F32)

    @pl.when(s == 0)
    def _():
        ext[:RIM, :] = jnp.zeros((RIM, chans), F32)

    def share_squares(k, total):
        line = jnp.transpose(jnp.broadcast_to(total, (block, 128)))[:8]
        ss_buf[k, m] = line
        for j in range(1, tp):
            ss_copy(k, j, m).start()

    def row_factor(k, count):
        for j in range(1, tp):
            ss_copy(k, j, peer(j)).wait_recv()
        total = ss_buf[k, 0]
        for j in range(1, tp):
            total = total + ss_buf[k, j]
        line = lax.rsqrt(total[:1] * (1.0 / count) + EPS)
        return jnp.transpose(jnp.broadcast_to(line, (128, block)))[:, :1]

    position = s * block + lax.broadcasted_iota(jnp.int32, (block, 1), 0)
    since = position.astype(F32) + 1.0
    square_total = jnp.zeros((block, 1), F32)
    pw = 128
    means = []
    for c0 in range(0, chans, pw):
        current = ext[:, c0 : c0 + pw]
        channel = c0 + lax.broadcasted_iota(jnp.int32, (1, pw), 1)
        group = m * groups + channel // GROUP_DIM
        kind = lax.rem(group, 4)
        total = current
        chosen = jnp.zeros((block, pw), F32)
        for level in range(4):
            total = total + pltpu.roll(total, 1 << level, 0)
            share = 1.0 / jnp.minimum(since, float(2 << level))
            chosen = jnp.where(kind == level, total[RIM:] * share, chosen)
        means.append((chosen - current[RIM:]).astype(BF16))
    pooled = dot(jnp.concatenate(means, axis=1) if len(means) > 1 else means[0], blockdiag[...])
    pooled = pooled * scale[...]
    pooled_ref[...] = pooled
    share_squares(0, jnp.sum(pooled * pooled, axis=1, keepdims=True))

    for j in range(1, tp):
        for c in f_copy(s, j, peer(j)):
            c.wait_recv()
    expand(s)
    for h in range(heads):
        attend(h, True)

    pool_factor = row_factor(0, GROUPS * GROUP_DIM)
    mixed[...] = (pooled_ref[...] * pool_factor * pool_gain[...]).astype(BF16)
    loads["po"].wait()
    pool_mixed = mixed[...]

    def pool_chunk(c, carry):
        at = pl.multiple_of(c * cw, 128)
        acc_pool[:, pl.ds(at, cw)] = dot(pool_mixed, pool_out[:, pl.ds(at, cw)])
        return carry

    lax.fori_loop(0, chunks, pool_chunk, 0)

    def earlier(d, carry):
        src = s - d
        for c in z_copy(0, src):
            c.wait_recv()
        for j in range(1, tp):
            for c in f_copy(src, j, m):
                c.start()
        for j in range(1, tp):
            for c in f_copy(src, j, peer(j)):
                c.wait_recv()
        expand(src)
        for h in range(heads):
            attend(h, False)
        return carry

    lax.fori_loop(1, s + 1, earlier, 0)

    loads["ag"].wait()
    square_total = jnp.zeros((block, 1), F32)
    for h in range(heads):
        lo = h * VALUE_DIM
        one = acc[h, :, :VALUE_DIM] / acc[h, :, VALUE_DIM:]
        square_total = square_total + jnp.sum(one * one, axis=1, keepdims=True)
        mixed[:, lo : lo + VALUE_DIM] = (one * att_gain[:, lo : lo + VALUE_DIM]).astype(BF16)
    share_squares(1, square_total)
    loads["ao"].wait()
    factor_att = row_factor(1, HEADS * VALUE_DIM)
    att_mixed = mixed[...]
    for c in range(chunks):
        lo = c * cw
        part = dot(att_mixed, att_out[:, lo : lo + cw]) * factor_att + acc_pool[:, lo : lo + cw]
        send_buf[c] = part.astype(BF16).reshape(tp, rows, cw)
        for j in range(1, tp):
            out_copy(c, j, m).start()
    for c in range(chunks):
        total = send_buf[c, m].astype(F32)
        for j in range(1, tp):
            out_copy(c, j, peer(j)).wait_recv()
            total = total + recv_buf[c, peer(j)].astype(F32)
        out_ref[:, c * cw : (c + 1) * cw] = total.astype(BF16)

    for j in range(1, tp):
        tok_copy(j, m).wait_send()
        for k in range(2):
            ss_copy(k, j, m).wait_send()
        for c in range(chunks):
            out_copy(c, j, m).wait_send()
    for d in range(1, sp):
        @pl.when(s + d < sp)
        def _():
            for c in z_copy(d, s):
                c.wait_send()

    @pl.when(s + 1 < sp)
    def _():
        rim_copy().wait_send()

    def drain(src, carry):
        for j in range(1, tp):
            for c in f_copy(src, j, m):
                c.wait_send()
        return carry

    lax.fori_loop(0, s + 1, drain, 0)


def turn_tables(length):
    steps = np.arange(HALF, dtype=np.float32) / np.float32(HALF)
    inv_freq = np.float32(1.0) / np.power(np.float32(THETA), steps).astype(np.float32)
    angle = inv_freq[:, None] * np.arange(length, dtype=np.float32)[None, :]
    angle = angle.astype(np.float32).astype(np.float64)
    return np.cos(angle).astype(np.float32), np.sin(angle).astype(np.float32)


def local(
    tokens, input_gain, query_weight, latent_down, rotary_down, pool_down, key_up, value_up,
    query_gain, key_gain, pool_weight, pool_scale, attention_gain, pool_gain, attention_out, pool_out,
):
    sp = lax.axis_size("sp")
    tp = lax.axis_size("tp")
    _, rows, width = tokens.shape
    block = rows * tp
    heads = HEADS // tp
    groups = GROUPS // tp
    chans = groups * GROUP_DIM
    cosine, sine = turn_tables(block * sp)
    chunks = 4
    cw = width // chunks
    line = lambda v: v.reshape(1, -1)
    operands = [
        tokens[0], line(input_gain), query_weight, latent_down, rotary_down, pool_down, key_up, value_up,
        line(query_gain), line(key_gain), pool_weight, line(pool_scale), line(attention_gain),
        line(pool_gain), attention_out, pool_out, jnp.asarray(cosine), jnp.asarray(sine),
    ]
    V = pltpu.VMEM
    D = pltpu.SemaphoreType.DMA
    held = [V(o.shape, o.dtype) for o in operands]
    held[0] = V((tp, rows, width), BF16)
    held[7] = V((KV_LATENT, heads * VALUE_DIM), BF16)
    held[10] = V((groups, GROUP_DIM, GROUP_DIM), BF16)
    scratch = held + [
        V((tp, rows, width), BF16),
        V((HEADS * NOPE_DIM, KV_LATENT), BF16),
        V((sp, tp, rows, KV_LATENT), BF16),
        V((sp, tp, ROPE_DIM, rows), BF16),
        V((heads, block, 128), BF16),
        V((heads, 128, block), BF16),
        V((heads, block, 2 * VALUE_DIM), BF16),
        V((heads, block, 2 * VALUE_DIM), F32),
        V((block + RIM, chans), F32),
        V((RIM, chans), BF16),
        V((RIM, chans), BF16),
        V((chans, chans), BF16),
        V((block, chans), F32),
        V((block, width), F32),
        V((2, tp, 8, block), F32),
        V((block, chans), BF16),
        V((chunks, tp, rows, cw), BF16),
        V((chunks, tp, rows, cw), BF16),
        D((len(operands),)),
        D((tp,)), D((tp,)),
        D((sp, 2)), D((sp, 2)),
        D((sp, tp, 2)), D((sp, tp, 2)),
        D((1,)), D((1,)),
        D((2, tp)), D((2, tp)),
        D((chunks, tp)), D((chunks, tp)),
    ]
    out = pl.pallas_call(
        functools.partial(kernel, sp, tp),
        out_shape=jax.ShapeDtypeStruct((rows, width), BF16),
        in_specs=[pl.BlockSpec(memory_space=pl.ANY)] * len(operands),
        out_specs=pl.BlockSpec(memory_space=pltpu.VMEM),
        scratch_shapes=scratch,
        compiler_params=pltpu.CompilerParams(
            collective_id=0, has_side_effects=True, vmem_limit_bytes=58 * 1024 * 1024
        ),
    )(*operands)
    return out[None]


def solution(mesh):
    placed = (
        P("fs", ("sp", "tp"), None), P(), P(None, "tp"), P(), P(), P(None, "tp"), P(), P(),
        P(), P(), P(), P("tp"), P("tp"), P("tp"), P("tp", None), P("tp", None),
    )
    return jax.shard_map(
        local, mesh=mesh, in_specs=placed, out_specs=P("fs", ("sp", "tp"), None), check_vma=False
    )
```

time: 159 us -> 39.4 us (0.25)
  the two profiles are of different devices: /device:TPU:25 before, /device:TPU:17 now
where the time goes in v1:
time: 39.4 us; the launch traced here: 39.2 us
  Pallas kernels  35 us (89%)
  local copies, waits for them, and re-layouts  4.21 us (11%)
    pallas_call x1, Pallas kernels, local(): pl.pallas_call(functools.partial(kernel, sp, tp), out_shape=jax.ShapeDtyp...  35 us
    unnamed x2, local copies, waits for them, and re-layouts  4.21 us

profile of v1, /device:TPU:17, one launch (start us, length us, event | category | flops | bytes accessed | tf_op | source)
XLA Modules:
  0.0 39.2 jit_solution(5326133903432820929)
XLA Ops:
  0.0 1.9 %copy.19.rotary_w_h = bf16[2048,32]{1,0:T(8,128)(2,1)} copy(bf16[2048,32]{0,1:T(8,128)(2,1)} %param.22) | data formatting | bytes 262144 | tf_op args[4]
  1.9 35.0 %shard_map.172 = bf16[256,2048]{1,0:T(8,128)(2,1)} custom-call(bf16[256,2048]{1,0:T(8,128)(2,1)} %bitcast.9, f32[1,2048]{1,0:T(1,128)} %bitcast.10, bf16[2048,384]{1,0:T(8,128)(2,1)} %query_w_h.1, bf16[2048,256]{1,0:T(8,128)(2,1)} %latent_w_h.1, bf16[2048,32]{1,0:T(8,128)(2,1)} %copy.19.rotary_w_h, bf16[2048,512]{1,0:T(8,128)(2,1)} %pool_w_h.1, ...), custom_call_target="tpu_custom_call" | custom-call | tf_op jit(solution)/shard_map/pallas_call | solution.py:452
  36.9 2.3 %copy.21 = bf16[1,256,2048]{2,1,0:T(8,128)(2,1)} copy(bf16[1,256,2048]{2,1,0:T(8,128)(2,1)} %bitcast.8) | data formatting | bytes 2097152

commit v2 on v1

--- a/solution.py
+++ b/solution.py
@@ -42,9 +42,9 @@
     out_ref,
     x_all, input_gain, query_w, latent_w, rotary_w, pool_w, key_up, value_up,
     query_gain, key_gain, mix_w, scale, att_gain, pool_gain, att_out, pool_out, cos_t, sin_t,
-    normed, key_up_t, lat_buf, rot_buf, queries, keys_t, vals, acc, ext, rim_out, rim_in, blockdiag,
+    normed, key_up_t, lat_buf, rot_buf, queries, keys_t, vals, acc, ext, tail_in, blockdiag,
     pooled_ref, acc_pool, ss_buf, mixed, send_buf, recv_buf,
-    load_sem, tok_send, tok_recv, z_send, z_recv, f_send, f_recv, rim_send, rim_recv,
+    load_sem, tok_send, tok_recv, z_send, z_recv, f_send, f_recv, tail_send, tail_recv,
     ss_send, ss_recv, out_send, out_recv,
 ):
     s = lax.axis_index("sp")
@@ -89,8 +89,14 @@
     for j in range(1, tp):
         pl.semaphore_signal(barrier, inc=1, device_id={"tp": peer(j)}, device_id_type=MESH)
     for d in range(1, sp):
-        pl.semaphore_signal(barrier, inc=1, device_id={"sp": lax.rem(s + d, sp)}, device_id_type=MESH)
-    pl.semaphore_wait(barrier, tp - 1 + sp - 1)
+        @pl.when(s >= d)
+        def _():
+            pl.semaphore_signal(barrier, inc=1, device_id={"sp": lax.rem(s + sp - d, sp)}, device_id_type=MESH)
+
+    @pl.when(jnp.logical_and(s > 0, m < tp - 1))
+    def _():
+        where = {"sp": lax.rem(s + sp - 1, sp), "tp": tp - 1}
+        pl.semaphore_signal(barrier, inc=1, device_id=where, device_id_type=MESH)
 
     def remote(src, dst, ssem, rsem, where):
         return pltpu.make_async_remote_copy(
@@ -100,12 +106,32 @@
     def tok_copy(j, owner):
         return remote(tokens_h, x_all.at[owner], tok_send.at[j], tok_recv.at[owner], {"tp": peer(j)})
 
-    def z_copy(d, src):
-        where = {"sp": lax.rem(s + d, sp)}
+    def z_copy(hop, src):
+        where = {"sp": lax.rem(s + hop + 1, sp)}
         return [
-            remote(buf.at[src, m], buf.at[src, m], z_send.at[d, k], z_recv.at[src, k], where)
+            remote(buf.at[src, m], buf.at[src, m], z_send.at[src, hop, k], z_recv.at[src, k], where)
             for k, buf in enumerate((lat_buf, rot_buf))
         ]
+
+    odd = lax.rem(s, 2)
+    hops = ((0, s + 1 < sp), (1, jnp.logical_and(s + 2 < sp, odd == 0)))
+
+    def relays(d):
+        return jnp.logical_and(s + 1 < sp, jnp.logical_or(odd == 0, d > 1))
+
+    def arrive(d):
+        src = s - d
+        for c in z_copy(0, src):
+            c.wait_recv()
+
+        @pl.when(relays(d))
+        def _():
+            for c in z_copy(0, src):
+                c.start()
+
+        for j in range(1, tp):
+            for c in f_copy(src, j, m):
+                c.start()
 
     def f_copy(src, j, owner):
         where = {"tp": peer(j)}
@@ -114,8 +140,9 @@
             for k, buf in enumerate((lat_buf, rot_buf))
         ]
 
-    def rim_copy():
-        return remote(rim_out, rim_in, rim_send.at[0], rim_recv.at[0], {"sp": lax.rem(s + 1, sp)})
+    def tail_copy(j):
+        where = {"sp": lax.rem(s + 1, sp), "tp": j}
+        return remote(tokens_h.at[rows - RIM :, :], tail_in, tail_send.at[j], tail_recv.at[0], where)
 
     def ss_copy(k, j, owner):
         return remote(ss_buf.at[k, owner], ss_buf.at[k, owner], ss_send.at[k, j], ss_recv.at[k, owner], {"tp": peer(j)})
@@ -123,17 +150,24 @@
     def out_copy(c, j, owner):
         return remote(send_buf.at[c, peer(j)], recv_buf.at[c, owner], out_send.at[c, j], out_recv.at[c, owner], {"tp": peer(j)})
 
-    for j in range(1, tp):
-        tok_copy(j, m).start()
-
+    apart = rows % 128 == 0
     step = min(64, rows)
 
+    def slot_of(piece):
+        return lax.rem(piece - m + tp, tp) if apart else piece
+
+    def norm_rows(x):
+        x = x.astype(F32)
+        r = lax.rsqrt(jnp.mean(x * x, axis=-1, keepdims=True) + EPS)
+        return (x * r * input_gain[...]).astype(BF16)
+
     def norm_piece(piece):
+        first = slot_of(piece) * rows
+
         def body(i, carry):
             at = pl.multiple_of(i * step, step)
-            x = x_all[piece, pl.ds(at, step), :].astype(F32)
-            r = lax.rsqrt(jnp.mean(x * x, axis=-1, keepdims=True) + EPS)
-            normed[piece, pl.ds(at, step), :] = (x * r * input_gain[...]).astype(BF16)
+            to = pl.multiple_of(first + i * step, step)
+            normed[pl.ds(to, step), :] = norm_rows(x_all[piece, pl.ds(at, step), :])
             return carry
 
         lax.fori_loop(0, rows // step, body, 0)
@@ -141,57 +175,88 @@
     loads["x"].wait()
     loads["ig"].wait()
     norm_piece(m)
+
+    later = sp - 1 - s
+    sends_tail = lax.div(m + 1, tp) * lax.div(later + max(sp - 2, 0), max(sp - 1, 1))
+    pl.semaphore_wait(barrier, tp - 1 + later + sends_tail * (tp - 1))
+
+    for j in range(1, tp):
+        tok_copy(j, m).start()
+
+    @pl.when(jnp.logical_and(s + 1 < sp, m == tp - 1))
+    def _():
+        for j in range(tp):
+            tail_copy(j).start()
+
     loads["lw"].wait()
     loads["rw"].wait()
-    own = normed[m]
+    own = normed[pl.ds(pl.multiple_of(slot_of(m) * rows, rows), rows), :]
+    rot_buf[s, m] = lax.dot_general(
+        rotary_w[...], own, (((1,), (1,)), ((), ())), preferred_element_type=F32
+    ).astype(BF16)
     lat_buf[s, m] = dot(own, latent_w[...]).astype(BF16)
-    rot = dot(own, rotary_w[...])
-    rot = jnp.concatenate([rot, jnp.zeros((rows, 128 - ROPE_DIM), F32)], axis=1)
-    rot_buf[s, m] = jnp.transpose(rot)[:ROPE_DIM].astype(BF16)
-    for d in range(1, sp):
-        @pl.when(s + d < sp)
+    for hop, wanted in hops:
+        @pl.when(wanted)
         def _():
-            for c in z_copy(d, s):
+            for c in z_copy(hop, s):
                 c.start()
     for j in range(1, tp):
         for c in f_copy(s, j, m):
             c.start()
 
-    for j in range(1, tp):
-        tok_copy(j, peer(j)).wait_recv()
-        norm_piece(peer(j))
-
-    full = normed[...].reshape(block, width)
-    loads["pw"].wait()
-    pool_in = dot(full, pool_w[...]).astype(BF16)
-    ext[RIM:, :] = pool_in.astype(F32)
-    rim_out[...] = pool_in[block - RIM :, :]
-
-    @pl.when(s + 1 < sp)
-    def _():
-        rim_copy().start()
-
     loads["qw"].wait()
     loads["qg"].wait()
     loads["cos"].wait()
     loads["sin"].wait()
-    query_t = jnp.transpose(dot(full, query_w[...]))
     factor = math.log2(math.e) / math.sqrt(QK_DIM)
     gain_q = column_of(query_gain[...], QK_DIM) * factor
-    at = pl.multiple_of(s * block, 128)
-    cosine = cos_t[:, pl.ds(at, block)]
-    sine = sin_t[:, pl.ds(at, block)]
-    pad = jnp.zeros((128 - QK_DIM, block), F32)
-    for h in range(heads):
-        u = query_t[h * QK_DIM : (h + 1) * QK_DIM]
-        r = lax.rsqrt(jnp.sum(u * u, axis=0, keepdims=True) * (1.0 / QK_DIM) + EPS)
-        n = u * r * gain_q
-        a = n[NOPE_DIM : NOPE_DIM + HALF]
-        b = n[NOPE_DIM + HALF :]
-        turned = jnp.concatenate(
-            [n[:NOPE_DIM], a * cosine - b * sine, b * cosine + a * sine, pad], axis=0
-        )
-        queries[h] = jnp.transpose(turned).astype(BF16)
+
+    def project(slot, at, count, last):
+        offset = slot * rows
+        query_t = jnp.transpose(dot(normed[offset : offset + count, :], query_w[...]))
+        first = pl.multiple_of(s * block + at, 128)
+        cosine = cos_t[:, pl.ds(first, count)]
+        sine = sin_t[:, pl.ds(first, count)]
+        pad = jnp.zeros((128 - QK_DIM, count), F32)
+        for h in range(heads):
+            u = query_t[h * QK_DIM : (h + 1) * QK_DIM]
+            r = lax.rsqrt(jnp.sum(u * u, axis=0, keepdims=True) * (1.0 / QK_DIM) + EPS)
+            n = u * r * gain_q
+            a = n[NOPE_DIM : NOPE_DIM + HALF]
+            b = n[NOPE_DIM + HALF :]
+            turned = jnp.concatenate(
+                [n[:NOPE_DIM], a * cosine - b * sine, b * cosine + a * sine, pad], axis=0
+            )
+            queries[h, pl.ds(at, count), :] = jnp.transpose(turned).astype(BF16)
+        taken = count
+        if last:
+            @pl.when(s > 0)
+            def _():
+                tail_copy(0).wait_recv()
+                normed[block:, :] = norm_rows(tail_in[...])
+
+            @pl.when(s == 0)
+            def _():
+                normed[block:, :] = jnp.zeros((RIM, width), BF16)
+
+            taken = count + RIM
+        pool_in = dot(normed[offset : offset + taken, :], pool_w[...]).astype(BF16).astype(F32)
+        ext[pl.ds(pl.multiple_of(RIM + at, RIM), count), :] = pool_in[:count]
+        if last:
+            ext[:RIM, :] = pool_in[count:]
+
+    loads["pw"].wait()
+    if apart:
+        for j in range(tp):
+            if j > 0:
+                tok_copy(j, peer(j)).wait_recv()
+                norm_piece(peer(j))
+            project(j, pl.multiple_of(peer(j) * rows, rows), rows, j == tp - 1)
+    else:
+        for j in range(1, tp):
+            tok_copy(j, peer(j)).wait_recv()
+            norm_piece(peer(j))
+        project(0, 0, block, True)
 
     loads["ku"].wait()
     key_up_t[...] = jnp.transpose(key_up[...].astype(F32)).astype(BF16)
@@ -257,15 +322,6 @@
         lo = g * GROUP_DIM
         blockdiag[lo : lo + GROUP_DIM, lo : lo + GROUP_DIM] = mix_w[g]
 
-    @pl.when(s > 0)
-    def _():
-        rim_copy().wait_recv()
-        ext[:RIM, :] = rim_in[...].astype(F32)
-
-    @pl.when(s == 0)
-    def _():
-        ext[:RIM, :] = jnp.zeros((RIM, chans), F32)
-
     def share_squares(k, total):
         line = jnp.transpose(jnp.broadcast_to(total, (block, 128)))[:8]
         ss_buf[k, m] = line
@@ -303,6 +359,10 @@
     pooled_ref[...] = pooled
     share_squares(0, jnp.sum(pooled * pooled, axis=1, keepdims=True))
 
+    @pl.when(s > 0)
+    def _():
+        arrive(1)
+
     for j in range(1, tp):
         for c in f_copy(s, j, peer(j)):
             c.wait_recv()
@@ -310,6 +370,10 @@
     for h in range(heads):
         attend(h, True)
 
+    @pl.when(s > 1)
+    def _():
+        arrive(2)
+
     pool_factor = row_factor(0, GROUPS * GROUP_DIM)
     mixed[...] = (pooled_ref[...] * pool_factor * pool_gain[...]).astype(BF16)
     loads["po"].wait()
@@ -324,17 +388,17 @@
 
     def earlier(d, carry):
         src = s - d
-        for c in z_copy(0, src):
-            c.wait_recv()
-        for j in range(1, tp):
-            for c in f_copy(src, j, m):
-                c.start()
         for j in range(1, tp):
             for c in f_copy(src, j, peer(j)):
                 c.wait_recv()
         expand(src)
         for h in range(heads):
             attend(h, False)
+
+        @pl.when(jnp.logical_and(d > 1, d < s))
+        def _():
+            arrive(d + 1)
+
         return carry
 
     lax.fori_loop(1, s + 1, earlier, 0)
@@ -369,15 +433,26 @@
             ss_copy(k, j, m).wait_send()
         for c in range(chunks):
             out_copy(c, j, m).wait_send()
-    for d in range(1, sp):
-        @pl.when(s + d < sp)
+    for hop, wanted in hops:
+        @pl.when(wanted)
         def _():
-            for c in z_copy(d, s):
+            for c in z_copy(hop, s):
                 c.wait_send()
 
-    @pl.when(s + 1 < sp)
+    def drain_relay(d, carry):
+        @pl.when(relays(d))
+        def _():
+            for c in z_copy(0, s - d):
+                c.wait_send()
+
+        return carry
+
+    lax.fori_loop(1, s + 1, drain_relay, 0)
+
+    @pl.when(jnp.logical_and(s + 1 < sp, m == tp - 1))
     def _():
-        rim_copy().wait_send()
+        for j in range(tp):
+            tail_copy(j).wait_send()
 
     def drain(src, carry):
         for j in range(1, tp):
@@ -412,7 +487,7 @@
     cw = width // chunks
     line = lambda v: v.reshape(1, -1)
     operands = [
-        tokens[0], line(input_gain), query_weight, latent_down, rotary_down, pool_down, key_up, value_up,
+        tokens[0], line(input_gain), query_weight, latent_down, rotary_down.T, pool_down, key_up, value_up,
         line(query_gain), line(key_gain), pool_weight, line(pool_scale), line(attention_gain),
         line(pool_gain), attention_out, pool_out, jnp.asarray(cosine), jnp.asarray(sine),
     ]
@@ -423,7 +498,7 @@
     held[7] = V((KV_LATENT, heads * VALUE_DIM), BF16)
     held[10] = V((groups, GROUP_DIM, GROUP_DIM), BF16)
     scratch = held + [
-        V((tp, rows, width), BF16),
+        V((block + RIM, width), BF16),
         V((HEADS * NOPE_DIM, KV_LATENT), BF16),
         V((sp, tp, rows, KV_LATENT), BF16),
         V((sp, tp, ROPE_DIM, rows), BF16),
@@ -432,8 +507,7 @@
         V((heads, block, 2 * VALUE_DIM), BF16),
         V((heads, block, 2 * VALUE_DIM), F32),
         V((block + RIM, chans), F32),
-        V((RIM, chans), BF16),
-        V((RIM, chans), BF16),
+        V((RIM, width), BF16),
         V((chans, chans), BF16),
         V((block, chans), F32),
         V((block, width), F32),
@@ -443,20 +517,20 @@
         V((chunks, tp, rows, cw), BF16),
         D((len(operands),)),
         D((tp,)), D((tp,)),
-        D((sp, 2)), D((sp, 2)),
+        D((sp, 2, 2)), D((sp, 2)),
         D((sp, tp, 2)), D((sp, tp, 2)),
-        D((1,)), D((1,)),
+        D((tp,)), D((1,)),
         D((2, tp)), D((2, tp)),
         D((chunks, tp)), D((chunks, tp)),
     ]
     out = pl.pallas_call(
         functools.partial(kernel, sp, tp),
-        out_shape=jax.ShapeDtypeStruct((rows, width), BF16),
-        in_specs=[pl.BlockSpec(memory_space=pl.ANY)] * len(operands),
+        out_shape=pltpu.VMEM((rows, width), BF16),
+        in_specs=[pl.BlockSpec(memory_space=pltpu.HBM)] * len(operands),
         out_specs=pl.BlockSpec(memory_space=pltpu.VMEM),
         scratch_shapes=scratch,
         compiler_params=pltpu.CompilerParams(
-            collective_id=0, has_side_effects=True, vmem_limit_bytes=58 * 1024 * 1024
+            collective_id=0, has_side_effects=True, vmem_limit_bytes=56 * 1024 * 1024
         ),
     )(*operands)
     return out[None]

time: 39.4 us -> 28.4 us (0.72)
  the two profiles are of different devices: /device:TPU:17 before, /device:TPU:25 now
where the time goes in v2:
time: 28.4 us; the launch traced here: 28.3 us
  Pallas kernels  27.3 us (96%)
  local copies, waits for them, and re-layouts  0.97 us (3%)
    pallas_call x1, Pallas kernels, local(): pl.pallas_call(functools.partial(kernel, sp, tp), out_shape=pltpu.VMEM((r...  27.3 us
    unnamed x1, local copies, waits for them, and re-layouts  0.97 us

profile of v2, /device:TPU:25, one launch (start us, length us, event | category | flops | bytes accessed | tf_op | source)
XLA Modules:
  0.0 28.3 jit_solution(10511762383696085219)
XLA Ops:
  0.0 27.3 %shard_map.172 = bf16[256,2048]{1,0:T(8,128)(2,1)S(1)} custom-call(bf16[256,2048]{1,0:T(8,128)(2,1)} %bitcast.10, f32[1,2048]{1,0:T(1,128)} %bitcast.12, bf16[2048,384]{1,0:T(8,128)(2,1)} %query_w_h.1, bf16[2048,256]{1,0:T(8,128)(2,1)} %latent_w_h.1, bf16[32,2048]{1,0:T(8,128)(2,1)} %bitcast.11, bf16[2048,512]{1,0:T(8,128)(2,1)} %pool_w_h.1, ...), custom_call_target="tpu_custom_call" | custom-call | tf_op jit(solution)/shard_map/pallas_call | solution.py:526
  27.3 1.0 %copy.20 = bf16[1,256,2048]{2,1,0:T(8,128)(2,1)} copy(bf16[1,256,2048]{2,1,0:T(8,128)(2,1)S(1)} %bitcast.9) | data formatting | bytes 2097152

commit v3 on v2

--- a/solution.py
+++ b/solution.py
@@ -82,8 +82,9 @@
         "ag": load(16, att_gain_h, att_gain),
         "ao": load(17, att_out_h, att_out),
     }
-    for item in loads.values():
-        item.start()
+    first_loads = ("x", "ig", "lw", "rw", "qw", "qg", "cos", "sin", "pw")
+    for name in first_loads:
+        loads[name].start()
 
     barrier = pltpu.get_barrier_semaphore()
     for j in range(1, tp):
@@ -203,6 +204,10 @@
     for j in range(1, tp):
         for c in f_copy(s, j, m):
             c.start()
+
+    for name, item in loads.items():
+        if name not in first_loads:
+            item.start()
 
     loads["qw"].wait()
     loads["qg"].wait()

time: 28.4 us -> 28.4 us (level)
  no operation moved by 1% of the time
where the time goes in v3:
time: 28.4 us; the launch traced here: 28.3 us
  Pallas kernels  27.3 us (96%)
  local copies, waits for them, and re-layouts  0.97 us (3%)
    pallas_call x1, Pallas kernels, local(): pl.pallas_call(functools.partial(kernel, sp, tp), out_shape=pltpu.VMEM((r...  27.3 us
    unnamed x1, local copies, waits for them, and re-layouts  0.97 us

profile of v3, /device:TPU:25, one launch (start us, length us, event | category | flops | bytes accessed | tf_op | source)
XLA Modules:
  0.0 28.3 jit_solution(17598489036859447974)
XLA Ops:
  0.0 27.3 %shard_map.172 = bf16[256,2048]{1,0:T(8,128)(2,1)S(1)} custom-call(bf16[256,2048]{1,0:T(8,128)(2,1)} %bitcast.10, f32[1,2048]{1,0:T(1,128)} %bitcast.12, bf16[2048,384]{1,0:T(8,128)(2,1)} %query_w_h.1, bf16[2048,256]{1,0:T(8,128)(2,1)} %latent_w_h.1, bf16[32,2048]{1,0:T(8,128)(2,1)} %bitcast.11, bf16[2048,512]{1,0:T(8,128)(2,1)} %pool_w_h.1, ...), custom_call_target="tpu_custom_call" | custom-call | tf_op jit(solution)/shard_map/pallas_call | solution.py:531
  27.3 1.0 %copy.20 = bf16[1,256,2048]{2,1,0:T(8,128)(2,1)} copy(bf16[1,256,2048]{2,1,0:T(8,128)(2,1)S(1)} %bitcast.9) | data formatting | bytes 2097152
